TPU v7x, 256 devices: a 4x2x16 block of a 4x16x16 slice. The times are simulated.
256 devices in a mesh: grp: 2 (over y), sp: 32 (over z, core), tp: 4 (over x).
Axes of the slice: x: 4, y: 2, z: 16, core: 2. Of those that a mesh axis runs over, the one named last changes fastest.
The devices are a block of a 4x16x16 slice.
Arguments:
- resid_in: bfloat16 [16384, 2048], P(('grp', 'sp', 'tp')), parts along dimension 0, may hold values from -3 to 3
- queries: bfloat16 [16384, 1024], P(('grp', 'sp'), 'tp'), parts along dimension 0, may hold values from -39 to 39
- keys: bfloat16 [16384, 1024], P(('grp', 'sp'), 'tp'), parts along dimension 0, may hold values from -6 to 6
- values: bfloat16 [16384, 1024], P(('grp', 'sp'), 'tp'), parts along dimension 0, may hold values from -12 to 12
- cum_gate: float32 [16384, 16], P('grp', 'tp'), parts along dimension 0, may hold values from -822 to 0, as said below
- w_out: bfloat16 [1024, 2048], replicated, may hold values from -0.1875 to 0.1875
- norm_gain: float32 [2048], replicated, may hold values from 0.1 to 1.9
- w_gate: bfloat16 [2048, 5632], P('sp', 'tp'), may hold values from -0.125 to 0.125
- w_up: bfloat16 [2048, 5632], P('sp', 'tp'), may hold values from -0.125 to 0.125
- w_down: bfloat16 [5632, 2048], P('tp', 'sp'), may hold values from -0.078125 to 0.078125
Outputs:
- resid_out: bfloat16 [16384, 2048], P(('grp', 'sp', 'tp')), parts along dimension 0
There are 2 independent parts, one for each index of `grp`. A program takes and returns all parts, laid end to end along the dimension named above; an argument that names none is the same for every part. Nothing has to cross between parts.
Inputs may be any that keep to these rules, and one draw needn't show every extreme that they name: `cum_gate`: in every head the values never rise from one position to the next, and the first is at most 0.
All inputs are finite; a program needn't handle non-finite values.
Results may differ from a plain program's by a relative error of at most 0.018.
Values may be sent and summed in bfloat16 or wider, within the bound.
A program may use at most 128 MiB of HBM per device.

v0:
```python
import math
import jax
import jax.numpy as jnp
from jax import lax
from jax.sharding import PartitionSpec as P

HEAD_DIM = 64


def sent_together(arrays, axis, dim, along):
    both = jnp.concatenate(arrays, axis=along)
    filled, at, finished = (lax.all_gather(both, axis, axis=dim, tiled=True), 0, [])
    for a in arrays:
        finished.append(lax.slice_in_dim(filled, at, at + a.shape[along], axis=along))
        at += a.shape[along]
    return tuple(finished)


def laid_out(blocks, dim):
    shape = list(blocks.shape[1:])
    shape[dim] *= blocks.shape[0]
    return jnp.moveaxis(blocks, 0, dim).reshape(shape)


def from_everyone(array, axis):
    length = lax.axis_size(axis)
    return lax.all_to_all(
        jnp.broadcast_to(array[None], (length, *array.shape)), axis, 0, 0, tiled=True
    )


def gathered_copies(array, axis, dim):
    return laid_out(from_everyone(array, axis), dim)


def turned_gather(arrays, axis, dims):
    turned = [jnp.moveaxis(a, dim, 0) for a, dim in zip(arrays, dims)]
    both = jnp.concatenate([t.reshape(len(t), -1) for t in turned], axis=1)
    filled, at, finished = (lax.all_gather(both, axis, axis=0, tiled=True), 0, [])
    for t, dim in zip(turned, dims):
        share = filled[:, at : at + t[0].size].reshape(-1, *t.shape[1:])
        finished.append(jnp.moveaxis(share, 0, dim))
        at += t[0].size
    return tuple(finished)


def in_blocks(array, dim, length):
    shape = array.shape
    blocks = array.reshape(*shape[:dim], length, shape[dim] // length, *shape[dim + 1 :])
    return jnp.moveaxis(blocks, dim, 0)


def sum_at_owner(array, axis, dim):
    length = lax.axis_size(axis)
    blocks = lax.all_to_all(in_blocks(array, dim, length), axis, 0, 0, tiled=True)
    return jnp.sum(blocks.astype(jnp.float32), axis=0)


def on_device(resid_in, queries, keys, values, cum_gate, w_out, norm_gain, w_gate, w_up, w_down):
    tok_rows = queries.shape[0]
    local_heads = queries.shape[1] // HEAD_DIM
    scale = HEAD_DIM ** (-0.5)
    offset = lax.axis_index("sp") * tok_rows
    query_heads = queries.reshape(tok_rows, local_heads, HEAD_DIM)
    own_gate = lax.dynamic_slice_in_dim(cum_gate, offset, tok_rows, 0).T
    query_pos = offset + jnp.arange(tok_rows, dtype=jnp.int32)
    last_pos = offset + tok_rows - 1
    initial = (
        jnp.full((local_heads, tok_rows), -1e30, jnp.float32),
        jnp.zeros((local_heads, tok_rows), jnp.float32),
        jnp.zeros((tok_rows, local_heads, HEAD_DIM), jnp.float32),
    )
    key_piece, value_piece = sent_together((keys, values), "sp", 0, 1)
    length = key_piece.shape[0]
    span = math.gcd(length, 512)

    def block(index, state):
        begin = index * span

        def work(inner):
            maxima, totals, summed = inner
            key_block = lax.dynamic_slice_in_dim(key_piece, index * span, span, 0).reshape(
                span, local_heads, HEAD_DIM
            )
            value_block_rows = lax.dynamic_slice_in_dim(value_piece, index * span, span, 0).reshape(
                span, local_heads, HEAD_DIM
            )
            key_gate = lax.dynamic_slice_in_dim(cum_gate, begin, span, 0).T
            scores = (
                jnp.einsum(
                    "qhd,khd->hqk", query_heads, key_block, preferred_element_type=jnp.float32
                )
                * scale
            )
            scores = scores + own_gate[:, :, None] - key_gate[:, None, :]
            key_pos = begin + jnp.arange(span, dtype=jnp.int32)
            mask = (key_pos[None, :] <= query_pos[:, None])[None]
            scores = jnp.where(mask, scores, -1e30)
            new_max = jnp.maximum(maxima, jnp.max(scores, axis=-1))
            weights = jnp.where(mask, jnp.exp(scores - new_max[:, :, None]), 0.0)
            rescale = jnp.exp(maxima - new_max)
            totals = totals * rescale + jnp.sum(weights, axis=-1)
            product = jnp.einsum(
                "hqk,khd->qhd",
                weights.astype(jnp.bfloat16),
                value_block_rows,
                preferred_element_type=jnp.float32,
            )
            summed = summed * rescale.T[:, :, None] + product
            return (new_max, totals, summed)

        return lax.cond(begin <= last_pos, work, lambda inner: inner, state)

    maxima, totals, summed = lax.fori_loop(0, length // span, block, initial)
    attended = (
        (summed / totals.T[:, :, None])
        .reshape(tok_rows, local_heads * HEAD_DIM)
        .astype(jnp.bfloat16)
    )
    head_rows = lax.all_to_all(attended, "tp", split_axis=0, concat_axis=1, tiled=True)
    mixed = jnp.dot(head_rows, w_out, preferred_element_type=jnp.float32)
    resid = resid_in.astype(jnp.float32) + mixed
    normed = resid * lax.rsqrt(jnp.mean(resid * resid, axis=-1, keepdims=True) + 1e-06)
    normed = (normed * norm_gain).astype(jnp.bfloat16)
    all_rows = gathered_copies(normed, "tp", 0)
    full_gate, full_up, full_down = turned_gather((w_gate, w_up, w_down), "sp", (0, 0, 1))
    gate = jnp.dot(all_rows, full_gate, preferred_element_type=jnp.float32)
    up = jnp.dot(all_rows, full_up, preferred_element_type=jnp.float32)
    hidden = (jax.nn.silu(gate) * up).astype(jnp.bfloat16)
    terms = jnp.dot(hidden, full_down, preferred_element_type=jnp.float32)
    back = sum_at_owner(terms.astype(jnp.bfloat16), "tp", 0)
    return (resid + back).astype(jnp.bfloat16)


def solution(mesh):
    return jax.shard_map(
        on_device,
        mesh=mesh,
        in_specs=(
            P(("grp", "sp", "tp"), None),
            P(("grp", "sp"), "tp"),
            P(("grp", "sp"), "tp"),
            P(("grp", "sp"), "tp"),
            P("grp", "tp"),
            P(),
            P(),
            P("sp", "tp"),
            P("sp", "tp"),
            P("tp", "sp"),
        ),
        out_specs=P(("grp", "sp", "tp"), None),
        check_vma=False,
    )
```

profile of v0, /device:TPU:33, one launch (start us, length us, event | category | flops | bytes accessed | tf_op | source)
XLA Modules:
  0.0 264.1 jit_solution(7843677757114892416)
XLA Ops:
  6.5 0.0 copy-start.1
  6.5 0.0 all-gather.3.cloned.1.call-start
  6.6 1.0 copy.16
  7.6 1.0 copy.17
  8.6 0.7 pad_maximum_fusion.1
  9.3 0.1 all-gather.3.cloned.1.call-update
  9.4 0.1 all-gather.5.cloned.1.call-start
  9.5 2.0 pad_maximum_fusion
  11.4 0.1 all-gather.5.cloned.1.call-update
  11.5 0.0 copy-done.1
  11.5 0.1 copy.18
  11.6 0.7 dynamic-slice_bitcast_fusion.1
  12.3 106.1 %all-gather.3.cloned.1.call-done = bf16[8192,512]{0,1:T(8,128)(2,1)} async-done(((bf16[256,512]{0,1:T(8,128)(2,1)}), bf16[8192,512]{0,1:T(8,128)(2,1)}) %all-gather.3.cloned.1.call-update) | async-done | bytes 8388624 | tf_op jit(solution)/shard_map/all_gather | solution.py:12
  118.4 5.9 %fusion.36 = (bf16[8192,256]{0,1:T(8,128)(2,1)}, bf16[8192,256]{0,1:T(8,128)(2,1)}) fusion(bf16[8192,512]{0,1:T(8,128)(2,1)} %all-gather.3.cloned.1.call-done), kind=kLoop, calls=%fused_computation.47 | loop fusion | bytes 16777216 | tf_op jit(solution)/shard_map/slice | solution.py:14
  124.4 0.0 copy-start
  124.4 4.6 %while.18 = (s32[]{:T(128)}, f32[4,256]{1,0:T(4,128)S(1)}, f32[4,256]{1,0:T(4,128)S(1)}, f32[256,4,64]{0,2,1:T(8,128)S(1)}, s32[]{:T(128)}, /*index=5*/bf16[8192...) while((s32[]{:T(128)}, f32[4,256]{1,0:T(4,128)S(1)}, ...), condition=%wide.region_5.6_spmd.clone, body=%wide.region_0.5_spmd.clone.sunk | while | flops 140250880 | bytes 9146775 | solution.py:114
  124.4 3.7 %conditional.3 = ((f32[4,256]{1,0:T(4,128)S(1)}, f32[4,256]{1,0:T(4,128)S(1)}, f32[256,4,64]{0,2,1:T(8,128)S(1)})) conditional(s32[]{:T(128)} %convert_element_type.56, (f32[4,256]{1,0:T(4,128)S(1)}, f32[4,256]{1,0:T(4,128)S(1)}, f32[256,4,64]{0,2,1:T(8,128)S(1)}) %tuple.47, (s32[]{:T(128)}, s32[]{:T(128)}, s32[]{:T(128)}, ...), branch_computations={%region_1.0_spmd, %region_2.4_spmd} | conditional | flops 140250880 | bytes 9145472 | solution.py:112
  124.5 0.7 dynamic-slice_bitcast_fusion
  125.2 0.1 broadcast_compare_fusion
  125.3 1.1 constant_dynamic-slice_fusion
  126.4 0.7 fusion.35
  127.1 0.5 fusion.4
  127.7 0.4 fusion.3
  129.0 0.2 reshape.69
  129.1 0.2 copy.22
  129.3 8.7 %all_to_all.26 = bf16[4,64,256]{2,1,0:T(8,128)(2,1)S(1)} all-to-all(bf16[4,64,256]{2,1,0:T(8,128)(2,1)S(1)} %copy.22), channel_id=1, replica_groups=mesh['grp'=2,'sp'=32,'tp'=4] {'tp'}, dimensions={0} | all-to-all | bytes 262144 | tf_op jit(solution)/shard_map/all_to_all | solution.py:120
  138.0 0.0 copy-done
  138.0 0.0 copy-start.2
  138.0 3.2 %multiply_reduce_fusion = (f32[64]{0:T(128)S(1)}, f32[64,2048]{1,0:T(8,128)S(1)}) fusion(bf16[64,1024]{1,0:T(8,128)(2,1)S(1)} %bitcast.37, bf16[1024,2048]{1,0:T(8,128)(2,1)} %param.19, bf16[64,2048]{1,0:T(8,128)(2,1)S(1)} %copy-done), kind=kOutput, calls=%fused_computation.40 | convolution fusion | flops 268959680 | bytes 5112064 | tf_op jit(solution)/shard_map/dot_general | solution.py:121
  141.3 0.0 copy-done.2
  141.3 0.1 multiply_convert_fusion
  141.4 0.1 broadcast_in_dim.46
  141.5 16.0 %all_to_all.27 = bf16[4,64,2048]{2,1,0:T(8,128)(2,1)S(1)} all-to-all(bf16[4,64,2048]{2,1,0:T(8,128)(2,1)S(1)} %broadcast_in_dim.46), channel_id=1, replica_groups=mesh['grp'=2,'sp'=32,'tp'=4] {'tp'}, dimensions={0} | all-to-all | bytes 2097152 | tf_op jit(solution)/shard_map/all_to_all | solution.py:27
  157.5 66.6 %all-gather.5.cloned.1.call-done = bf16[2048,4224]{1,0:T(8,128)(2,1)} async-done(((bf16[64,4224]{1,0:T(8,128)(2,1)}), bf16[2048,4224]{1,0:T(8,128)(2,1)}) %all-gather.5.cloned.1.call-update) | async-done | bytes 17301520 | tf_op jit(solution)/shard_map/all_gather | solution.py:39
  224.1 5.6 %fusion.15 = f32[256,1408]{1,0:T(8,128)} fusion(bf16[256,2048]{1,0:T(8,128)(2,1)S(1)} %bitcast.33, bf16[2048,4224]{1,0:T(8,128)(2,1)} %all-gather.5.cloned.1.call-done), kind=kOutput, calls=%fused_computation.24 | convolution fusion | flops 1476395008 | bytes 8257536 | tf_op jit(solution)/shard_map/dot_general | solution.py:127
  229.7 8.2 %fusion.23 = bf16[256,2048]{1,0:T(8,128)(2,1)S(1)} fusion(bf16[2048,4224]{1,0:T(8,128)(2,1)} %all-gather.5.cloned.1.call-done, bf16[256,2048]{1,0:T(8,128)(2,1)S(1)} %bitcast.34, f32[256,1408]{1,0:T(8,128)} %fusion.15), kind=kOutput, calls=%fused_computation.28 | convolution fusion | flops 2955476992 | bytes 15073280 | tf_op jit(solution)/shard_map/dot_general | solution.py:130
  237.9 18.4 %all_to_all.28 = bf16[4,64,2048]{2,1,0:T(8,128)(2,1)S(1)} all-to-all(bf16[4,64,2048]{2,1,0:T(8,128)(2,1)S(1)} %bitcast.35), channel_id=1, replica_groups=mesh['grp'=2,'sp'=32,'tp'=4] {'tp'}, dimensions={0} | all-to-all | bytes 2097152 | tf_op jit(solution)/shard_map/all_to_all | solution.py:55
  256.3 0.2 convert_reduce_fusion
  256.5 0.8 add_convert_fusion
  (42 shorter events, 0.3 us)
Async XLA Ops:
  6.5 4.9 %copy-start.1 = (bf16[256,256]{1,0:T(8,128)(2,1)S(1)}, bf16[256,256]{1,0:T(8,128)(2,1)}, u32[]{:S(2)}) copy-start(bf16[256,256]{1,0:T(8,128)(2,1)} %param.15) | copy-start | bytes 393220
  6.5 111.8 %all-gather.3.cloned.1.call-start = ((), (), s32[]{:S(2)}) async-start(), calls=%async_computation.3 | async-start | bytes 8650752 | tf_op jit(solution)/shard_map/all_gather | solution.py:12
  9.4 214.7 %all-gather.5.cloned.1.call-start = ((), (), s32[]{:S(2)}) async-start(), calls=%async_computation.4 | async-start | bytes 17842176 | tf_op jit(solution)/shard_map/all_gather | solution.py:39
  124.4 13.7 %copy-start = (bf16[64,2048]{1,0:T(8,128)(2,1)S(1)}, bf16[64,2048]{1,0:T(8,128)(2,1)}, u32[]{:S(2)}) copy-start(bf16[64,2048]{1,0:T(8,128)(2,1)} %param.14) | copy-start | bytes 786436
  138.0 3.3 %copy-start.2 = (f32[2048]{0:T(1024)S(1)}, f32[2048]{0:T(1024)}, u32[]{:S(2)}) copy-start(f32[2048]{0:T(1024)} %param.20) | copy-start | bytes 24580
Sparse Core Ops, SparseCore 0:
  9.5 108.8 all-gather.2
  120.2 103.8 all-gather.4
where the time goes:
time: 265 us; the launch traced here: 264 us
  waiting for transfers between devices  173 us (65%)
  blocking collectives  43.1 us (16%)
  matrix products  18.3 us (7%)
  between operations  13.6 us (5%)
  local copies, waits for them, and re-layouts  11.1 us (4%)
  other arithmetic  4.31 us (2%)
    all_gather x1, waiting for transfers between devices, sent_together(): lax.all_gather(both, axis, axis=dim, tiled=True)  106 us
    all_gather x1, waiting for transfers between devices, turned_gather(): lax.all_gather(both, axis, axis=0, tiled=True)  66.6 us
    all_to_all x1, blocking collectives, sum_at_owner(): lax.all_to_all(in_blocks(array, dim, length), axis, 0, 0, tiled=True)  18.4 us
    all_to_all x1, blocking collectives, from_everyone(): lax.all_to_all(jnp.broadcast_to(array[None], (length, *array.shape)), axi...  16 us
    all_to_all x1, blocking collectives, on_device(): lax.all_to_all(attended, 'tp', split_axis=0, concat_axis=1, tiled=True)  8.67 us
    dot_general x1, matrix products, on_device(): terms = jnp.dot(hidden, full_down, preferred_element_type=jnp.float32)  8.19 us
    slice x1, local copies, waits for them, and re-layouts, sent_together(): lax.slice_in_dim(filled, at, at + a.shape[along], axis=along)  5.93 us
    dot_general x1, matrix products, on_device(): gate = jnp.dot(all_rows, full_gate, preferred_element_type=jnp.float32)  5.59 us
  transfers between devices with their start and end apart: 2, of which 2 were waited for; matrix products, arithmetic and copies ran while one was open for 6% of the time, Pallas kernels for 0%

commit v1 on v0

--- a/solution.py
+++ b/solution.py
@@ -5,6 +5,13 @@
 from jax.sharding import PartitionSpec as P
 
 HEAD_DIM = 64
+
+
+def swapped_in(x, mesh_axis, dim):
+    count = lax.axis_size(mesh_axis)
+    blocks = jnp.stack([x for _ in range(count)])
+    blocks = lax.all_to_all(blocks, mesh_axis, split_axis=0, concat_axis=0)
+    return jnp.concatenate(blocks, axis=dim)
 
 
 def sent_together(arrays, axis, dim, along):
@@ -36,7 +43,7 @@
 def turned_gather(arrays, axis, dims):
     turned = [jnp.moveaxis(a, dim, 0) for a, dim in zip(arrays, dims)]
     both = jnp.concatenate([t.reshape(len(t), -1) for t in turned], axis=1)
-    filled, at, finished = (lax.all_gather(both, axis, axis=0, tiled=True), 0, [])
+    filled, at, finished = (swapped_in(both, axis, 0), 0, [])
     for t, dim in zip(turned, dims):
         share = filled[:, at : at + t[0].size].reshape(-1, *t.shape[1:])
         finished.append(jnp.moveaxis(share, 0, dim))

time: 265 us -> 1020 us (3.85)
  blocking collectives: 43.1 us -> 840 us
  waiting for transfers between devices: 173 us -> 121 us
    all_to_all x1, blocking collectives: 16 us -> 814 us  [swapped_in(): blocks = lax.all_to_all(blocks, mesh_axis, split_axis=0, concat_axis=0)]
    all_gather x1 -> x0, waiting for transfers between devices: 66.6 us -> none  [turned_gather(): lax.all_gather(both, axis, axis=0, tiled=True)]
    all_to_all x0 -> x1, waiting for transfers between devices: none -> 13.3 us  [from_everyone(): lax.all_to_all(jnp.broadcast_to(array[None], (length, *array.shape)), axi...]
  transfers between devices with their start and end apart: 2 -> 2, of which waited for: 2 -> 2; matrix products, arithmetic and copies ran while one was open for 6% -> 0% of each run, Pallas kernels for 0% -> 0%
where the time goes in v1:
time: 1020 us
  blocking collectives  840 us (82%)
  waiting for transfers between devices  121 us (12%)
  local copies, waits for them, and re-layouts  20.8 us (2%)
  matrix products  15.6 us (2%)
  between operations  13.6 us (1%)
    all_to_all x1, blocking collectives, swapped_in(): blocks = lax.all_to_all(blocks, mesh_axis, split_axis=0, concat_axis=0)  814 us
    all_gather x1, waiting for transfers between devices, sent_together(): lax.all_gather(both, axis, axis=dim, tiled=True)  107 us
  transfers between devices with their start and end apart: 2, of which 2 were waited for; matrix products, arithmetic and copies ran while one was open for 0% of the time, Pallas kernels for 0%

profile of v1, /device:TPU:33, one launch (start us, length us, event | category | flops | bytes accessed | tf_op | source)
XLA Modules:
  0.0 1017.1 jit_solution(11812430874341051000)
XLA Ops:
  6.5 0.0 all-gather.2.cloned.1.call-start
  6.6 1.0 copy.17
  7.6 1.0 copy.16
  8.6 0.7 pad_maximum_fusion.1
  9.3 0.1 all-gather.2.cloned.1.call-update
  9.4 1.0 copy.18
  10.4 0.7 dynamic-slice_bitcast_fusion.1
  11.1 107.3 %all-gather.2.cloned.1.call-done = bf16[8192,512]{0,1:T(8,128)(2,1)} async-done(((bf16[256,512]{0,1:T(8,128)(2,1)}), bf16[8192,512]{0,1:T(8,128)(2,1)}) %all-gather.2.cloned.1.call-update) | async-done | bytes 8388624 | tf_op jit(solution)/shard_map/all_gather | solution.py:19
  118.4 5.9 fusion.36
  124.2 0.0 copy-start.1
  124.3 4.6 while.18
  124.3 3.7 conditional.3
  124.3 0.7 dynamic-slice_bitcast_fusion
  125.0 1.1 constant_dynamic-slice_fusion
  126.1 0.1 broadcast_compare_fusion
  126.3 0.7 fusion.35
  127.0 0.4 fusion.3
  127.4 0.5 fusion.4
  128.9 0.2 reshape.75
  129.0 0.2 copy.22
  129.2 8.6 all_to_all.31
  137.8 0.0 copy-done.1
  137.8 0.0 copy-start.5
  137.9 3.2 multiply_reduce_fusion
  141.0 0.0 copy-done.5
  141.0 0.0 copy-start.2
  141.1 0.0 copy-start.3
  141.1 0.0 copy-start.4
  141.1 0.1 multiply_convert_fusion
  141.2 1.1 broadcast_in_dim.46
  142.3 3.6 all-to-all-start.1
  145.9 0.0 copy-done.2
  145.9 0.0 copy-done.3
  145.9 0.0 copy-done.4
  146.0 13.3 %all-to-all-done.1 = bf16[4,64,2048]{2,1,0:T(8,128)(2,1)S(1)} async-done(((bf16[4,64,2048]{2,1,0:T(8,128)(2,1)}), bf16[4,64,2048]{2,1,0:T(8,128)(2,1)S(1)}, u32[]{:S(2)}, u32[]{:S(2)}) %all-to-all-start.1) | async-done | bytes 1048608 | tf_op jit(solution)/shard_map/all_to_all | solution.py:34
  159.3 2.1 stack.2
  161.4 813.8 %all_to_all.32 = bf16[32,64,4224]{2,1,0:T(8,128)(2,1)S(1)} all-to-all(bf16[32,64,4224]{2,1,0:T(8,128)(2,1)S(1)} %stack.2), channel_id=1, replica_groups=mesh['grp'=2,'sp'=32,'tp'=4] {'sp'}, dimensions={0} | all-to-all | bytes 34603008 | tf_op jit(solution)/shard_map/all_to_all | solution.py:13
  975.1 0.0 copy-start
  975.1 5.9 copy-done
  981.0 3.0 fusion.15
  984.0 8.2 fusion.23
  992.2 17.1 %all_to_all.33 = bf16[4,64,2048]{2,1,0:T(8,128)(2,1)S(1)} all-to-all(bf16[4,64,2048]{2,1,0:T(8,128)(2,1)S(1)} %bitcast.38), channel_id=1, replica_groups=mesh['grp'=2,'sp'=32,'tp'=4] {'tp'}, dimensions={0} | all-to-all | bytes 2097152 | tf_op jit(solution)/shard_map/all_to_all | solution.py:62
  1009.3 0.2 convert_reduce_fusion
  1009.5 0.8 add_convert_fusion
  (43 shorter events, 0.4 us)
Async XLA Ops:
  6.5 111.8 %all-gather.2.cloned.1.call-start = ((), (), s32[]{:S(2)}) async-start(), calls=%async_computation.4 | async-start | bytes 8650752 | tf_op jit(solution)/shard_map/all_gather | solution.py:19
  124.2 13.6 %copy-start.1 = (bf16[64,2048]{1,0:T(8,128)(2,1)S(1)}, bf16[64,2048]{1,0:T(8,128)(2,1)}, u32[]{:S(2)}) copy-start(bf16[64,2048]{1,0:T(8,128)(2,1)} %param.14) | copy-start | bytes 786436
  137.8 3.2 copy-start.5
  141.0 4.9 copy-start.2
  141.1 4.9 copy-start.3
  141.1 4.9 copy-start.4
  142.3 17.0 %all-to-all-start.1 = ((bf16[4,64,2048]{2,1,0:T(8,128)(2,1)}), bf16[4,64,2048]{2,1,0:T(8,128)(2,1)S(1)}, u32[]{:S(2)}, u32[]{:S(2)}) async-start(bf16[4,64,2048]{2,1,0:T(8,128)(2,1)} %broadcast_in_dim.46), calls=%async_computation.1 | async-start | bytes 2097152 | tf_op jit(solution)/shard_map/all_to_all | solution.py:34
  975.1 5.9 copy-start
Sparse Core Ops, SparseCore 0:
  9.5 108.8 all-gather.1
